TPU v7x, 32 devices: a whole 2x2x4 slice. The times are simulated.
32 devices in a mesh: fs: 8 (over z, y), tp: 4 (over x, core).
Axes of the slice: x: 2, y: 2, z: 4, core: 2. Of those that a mesh axis runs over, the one named last changes fastest.
Arguments:
- tokens: bfloat16 [6144, 2048], P(('fs', 'tp')), may hold values from -60 to 60
- norm_gain: float32 [2048], P('fs'), may hold values from 0.1 to 1.9
- gate_weight: float32 [2048, 5632], P('fs', 'tp'), may hold values from -0.125 to 0.125
- up_weight: float32 [2048, 5632], P('fs', 'tp'), may hold values from -0.125 to 0.125
- down_weight: float32 [2048, 5632], P('fs', 'tp'), may hold values from -0.078125 to 0.078125
Outputs:
- mixed_rows: bfloat16 [6144, 2048], P(('fs', 'tp'))
- gate_out: bfloat16 [2048, 5632], P(None, 'tp')
- up_out: bfloat16 [2048, 5632], P(None, 'tp')
- down_out: bfloat16 [2048, 5632], P(None, 'tp')
All inputs are finite; a program needn't handle non-finite values.
Results may differ from a plain program's by a relative error of at most 0.014.
Values may be sent and summed in bfloat16 or wider, within the bound.
A program may use at most 128 MiB of HBM per device.

v0:
```python
import jax
import jax.numpy as jnp
from jax import lax
from jax.sharding import PartitionSpec as P


def normalize(source):
    widened = source.astype(jnp.float32)
    return (widened * lax.rsqrt(jnp.mean(widened * widened, axis=1, keepdims=True) + 1e-06)).astype(
        jnp.bfloat16
    )


def shards(tokens, norm_gain, gate_weight, up_weight, down_weight):
    row_gain = norm_gain[:, None]
    gate_local = (gate_weight * row_gain).astype(jnp.bfloat16)
    up_local = (up_weight * row_gain).astype(jnp.bfloat16)
    down_local = down_weight.astype(jnp.bfloat16)
    normed = normalize(tokens)
    gathered = lax.all_gather(normed, "tp", axis=0, tiled=True)
    down_whole = lax.all_gather(down_local, "fs", axis=0, tiled=True)
    gate_piece = lax.all_gather(gate_local, "fs", axis=0, tiled=True)
    up_piece = lax.all_gather(up_local, "fs", axis=0, tiled=True)
    gate_acc = jnp.dot(gathered, gate_piece, preferred_element_type=jnp.float32)
    up_acc = jnp.dot(gathered, up_piece, preferred_element_type=jnp.float32)
    hidden = (jax.nn.silu(gate_acc) * up_acc).astype(jnp.bfloat16)
    partial_value = lax.dot_general(
        hidden, down_whole, (((1,), (1,)), ((), ())), preferred_element_type=jnp.float32
    )
    mixed_rows = lax.psum_scatter(
        lax.optimization_barrier(partial_value.astype(jnp.bfloat16))
        .astype(jnp.float32)
        .astype(jnp.bfloat16),
        "tp",
        scatter_dimension=0,
        tiled=True,
    )
    return (mixed_rows, gate_piece, up_piece, down_whole)


def solution(mesh):
    in_specs = (P(("fs", "tp"), None), P("fs"), P("fs", "tp"), P("fs", "tp"), P("fs", "tp"))
    out_specs = (P(("fs", "tp"), None), P(None, "tp"), P(None, "tp"), P(None, "tp"))
    return jax.shard_map(shards, mesh=mesh, in_specs=in_specs, out_specs=out_specs, check_vma=False)
```

profile of v0, /device:TPU:0, one launch (start us, length us, event | category | flops | bytes accessed | tf_op | source)
XLA Modules:
  0.0 397.9 jit_solution(9030108663980922372)
XLA Ops:
  7.2 0.0 copy-start
  7.2 0.0 all-gather.5.cloned.1.call-start
  7.2 1.5 fusion
  8.7 2.2 fusion.1
  10.9 0.0 all-gather.5.cloned.1.call-update
  10.9 0.0 all-gather.7.cloned.1.call-start
  11.0 3.2 multiply_convert_fusion.1
  14.2 0.0 all-gather.7.cloned.1.call-update
  14.2 0.0 all-gather.11.cloned.1.call-start
  14.2 0.0 copy-done
  14.2 0.9 convert_element_type.28
  15.2 0.0 all-gather.11.cloned.1.call-update
  15.2 0.0 all-gather.9.cloned.1.call-start
  15.3 0.5 all-gather.9.cloned.1.call-update
  15.8 0.0 reduce-scatter.2.cloned.1.call-start
  15.8 26.5 %all-gather.5.cloned.1.call-done = bf16[768,2048]{1,0:T(8,128)(2,1)} async-done(((bf16[192,2048]{1,0:T(8,128)(2,1)}), bf16[768,2048]{1,0:T(8,128)(2,1)}) %all-gather.5.cloned.1.call-update) | async-done | bytes 3145744 | tf_op jit(solution)/shard_map/all_gather | solution.py:20
  42.3 0.0 copy-start.1
  42.3 95.1 %all-gather.7.cloned.1.call-done = bf16[2048,1408]{1,0:T(8,128)(2,1)} async-done(((bf16[256,1408]{1,0:T(8,128)(2,1)}), bf16[2048,1408]{1,0:T(8,128)(2,1)}) %all-gather.7.cloned.1.call-update) | async-done | bytes 5767184 | tf_op jit(solution)/shard_map/all_gather | solution.py:22
  137.4 9.7 %fusion.3 = f32[768,1408]{1,0:T(8,128)} fusion(bf16[768,2048]{1,0:T(8,128)(2,1)} %all-gather.5.cloned.1.call-done, bf16[2048,1408]{1,0:T(8,128)(2,1)} %all-gather.7.cloned.1.call-done), kind=kOutput, calls=%fused_computation.10 | convolution fusion | flops 4429185024 | bytes 13238272 | tf_op jit(solution)/shard_map/dot_general | solution.py:24
  147.1 83.6 %all-gather.11.cloned.1.call-done = bf16[2048,1408]{1,0:T(8,128)(2,1)} async-done(((bf16[256,1408]{1,0:T(8,128)(2,1)}), bf16[2048,1408]{1,0:T(8,128)(2,1)}) %all-gather.11.cloned.1.call-update) | async-done | bytes 5767184 | tf_op jit(solution)/shard_map/all_gather | solution.py:21
  230.7 93.1 %all-gather.9.cloned.1.call-done = bf16[2048,1408]{1,0:T(8,128)(2,1)} async-done(((bf16[256,1408]{1,0:T(8,128)(2,1)}), bf16[2048,1408]{1,0:T(8,128)(2,1)}) %all-gather.9.cloned.1.call-update) | async-done | bytes 5767184 | tf_op jit(solution)/shard_map/all_gather | solution.py:23
  323.8 0.0 copy-done.1
  323.8 17.3 %convolution_convert_fusion = bf16[768,2048]{1,0:T(8,128)(2,1)} fusion(bf16[2048,1408]{1,0:T(8,128)(2,1)} %all-gather.11.cloned.1.call-done, f32[768,1408]{1,0:T(8,128)} %fusion.3, bf16[768,2048]{1,0:T(8,128)(2,1)S(1)} %copy-done.1, bf16[2048,1408]{1,0:T(8,128)(2,1)} %all-gather.9.cloned.1.call-done), kind=kOutput, calls=%fused_computation.1 | convolution fusion | flops 8866430976 | bytes 22151168 | tf_op jit(solution)/shard_map/dot_general | solution.py:27
  341.2 0.0 reduce-scatter.2.cloned.1.call-update
  341.2 36.2 %reduce-scatter.2.cloned.1.call-done = bf16[192,2048]{1,0:T(8,128)(2,1)} async-done(((bf16[768,2048]{1,0:T(8,128)(2,1)}), bf16[192,2048]{1,0:T(8,128)(2,1)}) %reduce-scatter.2.cloned.1.call-update) | async-done | bytes 786448 | tf_op jit(solution)/shard_map/reduce_scatter | solution.py:30
  377.4 0.0 slice-start
  377.4 5.7 %copy.12 = bf16[2048,1408]{1,0:T(8,128)(2,1)} copy(bf16[2048,1408]{1,0:T(8,128)(2,1)} %all-gather.7.cloned.1.call-done) | data formatting | bytes 11534336
  383.2 0.0 slice-start.1
  383.2 5.7 %copy.13 = bf16[2048,1408]{1,0:T(8,128)(2,1)} copy(bf16[2048,1408]{1,0:T(8,128)(2,1)} %all-gather.9.cloned.1.call-done) | data formatting | bytes 11534336
  388.9 0.0 slice-done
  388.9 0.0 slice-done.1
  388.9 2.5 copy.14
  (2 shorter events, 0.0 us)
Async XLA Ops:
  7.2 7.1 %copy-start = (f32[256,1408]{1,0:T(8,128)S(1)}, f32[256,1408]{1,0:T(8,128)}, u32[]{:S(2)}) copy-start(f32[256,1408]{1,0:T(8,128)} %param.9) | copy-start | bytes 4325380
  7.2 35.2 %all-gather.5.cloned.1.call-start = ((), (), s32[]{:S(2)}) async-start(), calls=%async_computation.1 | async-start | bytes 3932160 | tf_op jit(solution)/shard_map/all_gather | solution.py:20
  10.9 126.5 %all-gather.7.cloned.1.call-start = ((), (), s32[]{:S(2)}) async-start(), calls=%async_computation.2 | async-start | bytes 6488064 | tf_op jit(solution)/shard_map/all_gather | solution.py:22
  14.2 216.5 %all-gather.11.cloned.1.call-start = ((), (), s32[]{:S(2)}) async-start(), calls=%async_computation.4 | async-start | bytes 6488064 | tf_op jit(solution)/shard_map/all_gather | solution.py:21
  15.2 308.6 %all-gather.9.cloned.1.call-start = ((), (), s32[]{:S(2)}) async-start(), calls=%async_computation.3 | async-start | bytes 6488064 | tf_op jit(solution)/shard_map/all_gather | solution.py:23
  15.8 361.6 %reduce-scatter.2.cloned.1.call-start = ((), (), s32[]{:S(2)}) async-start(), calls=%async_computation.5 | async-start | bytes 3932160 | tf_op jit(solution)/shard_map/reduce_scatter | solution.py:30
  42.3 281.5 %copy-start.1 = (bf16[768,2048]{1,0:T(8,128)(2,1)S(1)}, bf16[768,2048]{1,0:T(8,128)(2,1)}, u32[]{:S(2)}) copy-start(bf16[768,2048]{1,0:T(8,128)(2,1)} %all-gather.5.cloned.1.call-done) | copy-start | bytes 9437188
  377.4 11.5 %slice-start = ((s8[5767168]{0:T(1024)(128)(4,1)}), s8[4194304]{0:T(1024)(128)(4,1)S(1)}, s32[]{:S(2)}) async-start(s8[5767168]{0:T(1024)(128)(4,1)} %bitcast.5), calls=%async_computation.6 | async-start | bytes 8388608
  383.2 5.7 %slice-start.1 = ((s8[5767168]{0:T(1024)(128)(4,1)}), s8[1572864]{0:T(1024)(128)(4,1)S(1)}, s32[]{:S(2)}) async-start(s8[5767168]{0:T(1024)(128)(4,1)} %bitcast.5), calls=%async_computation.7 | async-start | bytes 3145728
Sparse Core Ops, SparseCore 0:
  11.1 31.2 all-gather.4
  45.1 92.2 all-gather.6
  140.2 90.4 all-gather.10
  233.3 90.4 all-gather.8
  341.3 36.0 reduce-scatter.1
where the time goes:
time: 398 us
  waiting for transfers between devices  335 us (84%)
  matrix products  27 us (7%)
  local copies, waits for them, and re-layouts  14 us (4%)
  between operations  13.8 us (3%)
  other arithmetic  7.8 us (2%)
    all_gather x1, waiting for transfers between devices, shards(): gate_piece = lax.all_gather(gate_local, 'fs', axis=0, tiled=True)  95.1 us
    all_gather x1, waiting for transfers between devices, shards(): up_piece = lax.all_gather(up_local, 'fs', axis=0, tiled=True)  93.1 us
    all_gather x1, waiting for transfers between devices, shards(): down_whole = lax.all_gather(down_local, 'fs', axis=0, tiled=True)  83.6 us
    reduce_scatter x1, waiting for transfers between devices, shards(): lax.psum_scatter(lax.optimization_barrier(partial_value.astype(jnp.bfloat...  36.2 us
    all_gather x1, waiting for transfers between devices, shards(): gathered = lax.all_gather(normed, 'tp', axis=0, tiled=True)  26.5 us
    dot_general x1, matrix products, shards(): lax.dot_general(hidden, down_whole, (((1,), (1,)), ((), ())), preferred_e...  17.3 us
    unnamed x11, local copies, waits for them, and re-layouts  14 us
    dot_general x1, matrix products, shards(): gate_acc = jnp.dot(gathered, gate_piece, preferred_element_type=jnp.float32)  9.67 us
  transfers between devices with their start and end apart: 5, of which 5 were waited for; matrix products, arithmetic and copies ran while one was open for 3% of the time, Pallas kernels for 0%

commit v1 on v0

--- a/solution.py
+++ b/solution.py
@@ -19,8 +19,11 @@
     normed = normalize(tokens)
     gathered = lax.all_gather(normed, "tp", axis=0, tiled=True)
     down_whole = lax.all_gather(down_local, "fs", axis=0, tiled=True)
-    gate_piece = lax.all_gather(gate_local, "fs", axis=0, tiled=True)
-    up_piece = lax.all_gather(up_local, "fs", axis=0, tiled=True)
+    gate_piece, up_piece = jnp.split(
+        lax.all_gather(jnp.concatenate([gate_local, up_local], axis=1), "fs", axis=0, tiled=True),
+        [gate_local.shape[1]],
+        axis=1,
+    )
     gate_acc = jnp.dot(gathered, gate_piece, preferred_element_type=jnp.float32)
     up_acc = jnp.dot(gathered, up_piece, preferred_element_type=jnp.float32)
     hidden = (jax.nn.silu(gate_acc) * up_acc).astype(jnp.bfloat16)

time: 398 us -> 366 us (0.920)
  waiting for transfers between devices: 335 us -> 304 us
    all_gather x2 -> x1, waiting for transfers between devices: 188 us -> 164 us  [shards(): lax.all_gather(jnp.concatenate([gate_local, up_local], axis=1), 'fs', axi...]
    split x0 -> x1, local copies, waits for them, and re-layouts: none -> 9.89 us  [shards(): jnp.split(lax.all_gather(jnp.concatenate([gate_local, up_local], axis=1),...]
    unnamed x11 -> x7, local copies, waits for them, and re-layouts: 14 us -> 5.68 us
    all_gather x1, waiting for transfers between devices: 26.5 us -> 19 us  [shards(): gathered = lax.all_gather(normed, 'tp', axis=0, tiled=True)]
  transfers between devices with their start and end apart: 5 -> 4, of which waited for: 5 -> 4; matrix products, arithmetic and copies ran while one was open for 3% -> 6% of each run, Pallas kernels for 0% -> 0%
where the time goes in v1:
time: 366 us
  waiting for transfers between devices  304 us (83%)
  matrix products  27.1 us (7%)
  local copies, waits for them, and re-layouts  15.6 us (4%)
  between operations  13.8 us (4%)
  other arithmetic  5.54 us (2%)
    all_gather x1, waiting for transfers between devices, shards(): lax.all_gather(jnp.concatenate([gate_local, up_local], axis=1), 'fs', axi...  164 us
    all_gather x1, waiting for transfers between devices, shards(): down_whole = lax.all_gather(down_local, 'fs', axis=0, tiled=True)  84.7 us
    reduce_scatter x1, waiting for transfers between devices, shards(): lax.psum_scatter(lax.optimization_barrier(partial_value.astype(jnp.bfloat...  36.2 us
    all_gather x1, waiting for transfers between devices, shards(): gathered = lax.all_gather(normed, 'tp', axis=0, tiled=True)  19 us
    dot_general x1, matrix products, shards(): lax.dot_general(hidden, down_whole, (((1,), (1,)), ((), ())), preferred_e...  17.3 us
    split x1, local copies, waits for them, and re-layouts, shards(): jnp.split(lax.all_gather(jnp.concatenate([gate_local, up_local], axis=1),...  9.89 us
    dot_general x1, matrix products, shards(): gate_acc = jnp.dot(gathered, gate_piece, preferred_element_type=jnp.float32)  9.8 us
  transfers between devices with their start and end apart: 4, of which 4 were waited for; matrix products, arithmetic and copies ran while one was open for 6% of the time, Pallas kernels for 0%

profile of v1, /device:TPU:0, one launch (start us, length us, event | category | flops | bytes accessed | tf_op | source)
XLA Modules:
  0.0 365.8 jit_solution(17747635171327998706)
XLA Ops:
  7.2 0.0 all-gather.6.cloned.1.call-start
  7.2 2.1 multiply_convert_fusion.2
  9.3 0.0 copy-start
  9.3 0.0 copy-start.1
  9.3 1.2 pad_maximum_fusion
  10.5 0.0 all-gather.6.cloned.1.call-update
  10.5 0.0 all-gather.4.cloned.1.call-start
  10.6 0.1 copy-done
  10.7 0.2 fusion
  10.9 1.1 fusion.1
  12.0 0.0 all-gather.4.cloned.1.call-update
  12.0 0.0 all-gather.8.cloned.1.call-start
  12.1 0.0 copy-done.1
  12.1 0.9 convert_element_type.28
  13.0 0.0 all-gather.8.cloned.1.call-update
  13.0 0.0 reduce-scatter.2.cloned.1.call-start
  13.1 163.7 %all-gather.6.cloned.1.call-done = bf16[2048,2816]{1,0:T(8,128)(2,1)} async-done(((bf16[256,2816]{1,0:T(8,128)(2,1)}), bf16[2048,2816]{1,0:T(8,128)(2,1)}) %all-gather.6.cloned.1.call-update) | async-done | bytes 11534352 | tf_op jit(solution)/shard_map/all_gather | solution.py:23
  176.8 9.9 %fusion.3 = (bf16[2048,1408]{1,0:T(8,128)(2,1)}, bf16[2048,1408]{1,0:T(8,128)(2,1)}) fusion(bf16[2048,2816]{1,0:T(8,128)(2,1)} %all-gather.6.cloned.1.call-done), kind=kLoop, calls=%fused_computation.11 | loop fusion | bytes 23068672 | tf_op jit(solution)/shard_map/split | solution.py:22
  186.7 19.0 %all-gather.4.cloned.1.call-done = bf16[768,2048]{1,0:T(8,128)(2,1)} async-done(((bf16[192,2048]{1,0:T(8,128)(2,1)}), bf16[768,2048]{1,0:T(8,128)(2,1)}) %all-gather.4.cloned.1.call-update) | async-done | bytes 3145744 | tf_op jit(solution)/shard_map/all_gather | solution.py:20
  205.7 0.0 copy-start.2
  205.7 9.8 %fusion.4 = f32[768,1408]{1,0:T(8,128)} fusion(bf16[768,2048]{1,0:T(8,128)(2,1)} %all-gather.4.cloned.1.call-done, bf16[2048,1408]{1,0:T(8,128)(2,1)} %get-tuple-element.13), kind=kOutput, calls=%fused_computation.12 | convolution fusion | flops 4429185024 | bytes 13238272 | tf_op jit(solution)/shard_map/dot_general | solution.py:27
  215.5 84.7 %all-gather.8.cloned.1.call-done = bf16[2048,1408]{1,0:T(8,128)(2,1)} async-done(((bf16[256,1408]{1,0:T(8,128)(2,1)}), bf16[2048,1408]{1,0:T(8,128)(2,1)}) %all-gather.8.cloned.1.call-update) | async-done | bytes 5767184 | tf_op jit(solution)/shard_map/all_gather | solution.py:21
  300.2 0.0 copy-done.2
  300.2 17.3 %convolution_convert_fusion = bf16[768,2048]{1,0:T(8,128)(2,1)} fusion(bf16[2048,1408]{1,0:T(8,128)(2,1)} %all-gather.8.cloned.1.call-done, f32[768,1408]{1,0:T(8,128)} %fusion.4, bf16[768,2048]{1,0:T(8,128)(2,1)S(1)} %copy-done.2, bf16[2048,1408]{1,0:T(8,128)(2,1)} %get-tuple-element.14), kind=kOutput, calls=%fused_computation.1 | convolution fusion | flops 8866430976 | bytes 22151168 | tf_op jit(solution)/shard_map/dot_general | solution.py:30
  317.5 0.0 reduce-scatter.2.cloned.1.call-update
  317.5 36.2 %reduce-scatter.2.cloned.1.call-done = bf16[192,2048]{1,0:T(8,128)(2,1)} async-done(((bf16[768,2048]{1,0:T(8,128)(2,1)}), bf16[192,2048]{1,0:T(8,128)(2,1)}) %reduce-scatter.2.cloned.1.call-update) | async-done | bytes 786448 | tf_op jit(solution)/shard_map/reduce_scatter | solution.py:33
  353.7 5.6 %copy.10 = bf16[2048,1408]{1,0:T(8,128)(2,1)} copy(bf16[2048,1408]{1,0:T(8,128)(2,1)} %all-gather.8.cloned.1.call-done) | data formatting | bytes 11534336
  (1 shorter events, 0.0 us)
Async XLA Ops:
  7.2 169.6 %all-gather.6.cloned.1.call-start = ((), (), s32[]{:S(2)}) async-start(), calls=%async_computation.2 | async-start | bytes 12976128 | tf_op jit(solution)/shard_map/all_gather | solution.py:23
  9.3 1.4 copy-start
  9.3 2.8 copy-start.1
  10.5 195.1 %all-gather.4.cloned.1.call-start = ((), (), s32[]{:S(2)}) async-start(), calls=%async_computation.1 | async-start | bytes 3932160 | tf_op jit(solution)/shard_map/all_gather | solution.py:20
  12.0 288.2 %all-gather.8.cloned.1.call-start = ((), (), s32[]{:S(2)}) async-start(), calls=%async_computation.3 | async-start | bytes 6488064 | tf_op jit(solution)/shard_map/all_gather | solution.py:21
  13.0 340.7 %reduce-scatter.2.cloned.1.call-start = ((), (), s32[]{:S(2)}) async-start(), calls=%async_computation.4 | async-start | bytes 3932160 | tf_op jit(solution)/shard_map/reduce_scatter | solution.py:33
  205.7 94.5 %copy-start.2 = (bf16[768,2048]{1,0:T(8,128)(2,1)S(1)}, bf16[768,2048]{1,0:T(8,128)(2,1)}, u32[]{:S(2)}) copy-start(bf16[768,2048]{1,0:T(8,128)(2,1)} %all-gather.4.cloned.1.call-done) | copy-start | bytes 9437188
Sparse Core Ops, SparseCore 0:
  10.7 166.0 all-gather.5
  178.9 26.6 all-gather.3
  207.8 92.2 all-gather.7
  317.6 36.0 reduce-scatter.1
